TPU v7x, 32 devices: a whole 2x2x4 slice. The times are simulated.
32 devices in a mesh: ep: 4 (over z), tp: 8 (over y, x, core).
Axes of the slice: x: 2, y: 2, z: 4, core: 2. Of those that a mesh axis runs over, the one named last changes fastest.
Arguments:
- hidden_in: bfloat16 [48, 2048], P('ep', 'tp'), may hold values from -12 to 12
- state: float32 [48, 32, 128, 128], P('ep', 'tp'), may hold values from -3 to 3
- lower_bound: float32 [32, 128], P('tp'), may hold values from 0.05 to 0.95
- w_forget: bfloat16 [2048, 4096], P(None, 'tp'), may hold values from -0.125 to 0.125
- w_input: bfloat16 [2048, 4096], P(None, 'tp'), may hold values from -0.125 to 0.125
- w_query: bfloat16 [2048, 4096], P(None, 'tp'), may hold values from -0.125 to 0.125
- w_outgate: bfloat16 [2048, 4096], P(None, 'tp'), may hold values from -0.125 to 0.125
- head_gain: float32 [128], replicated, may hold values from 0.1 to 1.9
- w_out: bfloat16 [4096, 2048], P('tp'), may hold values from -0.125 to 0.125
- ln1_gain: float32 [2048], replicated, may hold values from 0.1 to 8
- ln1_bias: float32 [2048], replicated, may hold values from -1.5 to 1.5
- routes: int32 [48, 4], P('ep'), may hold values from 0 to 7, all different within a row; in each aligned block of 12 rows (0 to 11, 12 to 23, ...) at most 9 rows name the same one
- route_weights: float32 [48, 4], P('ep'), may hold values from 0.2 to 1.5
- exp_gate: bfloat16 [8, 2048, 4096], P('ep', None, 'tp'), may hold values from -0.125 to 0.125
- exp_up: bfloat16 [8, 2048, 4096], P('ep', None, 'tp'), may hold values from -0.125 to 0.125
- exp_down: bfloat16 [8, 4096, 2048], P('ep', 'tp'), may hold values from -0.125 to 0.125
- sh_gate: bfloat16 [2048, 512], P(None, 'tp'), may hold values from -0.125 to 0.125
- sh_up: bfloat16 [2048, 512], P(None, 'tp'), may hold values from -0.125 to 0.125
- sh_down: bfloat16 [512, 2048], P('tp'), may hold values from -0.25 to 0.25
- ln2_gain: float32 [2048], replicated, may hold values from 0.1 to 1.9
- ln2_bias: float32 [2048], replicated, may hold values from -1.5 to 1.5
Outputs:
- mixed_out: bfloat16 [48, 2048], P('ep', 'tp')
- new_state: float32 [48, 32, 128, 128], P('ep', 'tp')
Inputs may be any that keep to these rules, and one draw needn't show every extreme that they name: `routes`: each row names 4 different experts; among the rows of one index of ep (12 rows) no expert is named more than 9 times, a bound that some block reaches.
All inputs are finite; a program needn't handle non-finite values.
Results may differ from a plain program's by a relative error of at most 0.023.
Values may be sent and summed in bfloat16 or wider, within the bound.
A program may use at most 64 MiB of HBM per device.

v0:
```python
import jax
import jax.numpy as jnp
from jax import lax
from jax.sharding import PartitionSpec as P

EPS = 1e-05
ALPHA = 2.0**0.25


def rounded(value):
    return lax.optimization_barrier(value.astype(jnp.bfloat16)).astype(jnp.float32)


def local(
    hidden_in,
    state,
    lower_bound,
    w_forget,
    w_input,
    w_query,
    w_outgate,
    head_gain,
    w_out,
    ln1_gain,
    ln1_bias,
    routes,
    route_weights,
    exp_gate,
    exp_up,
    exp_down,
    sh_gate,
    sh_up,
    sh_down,
    ln2_gain,
    ln2_bias,
):
    n_tp = lax.axis_size("tp")
    n_ep = lax.axis_size("ep")
    seq_count = hidden_in.shape[0]
    col_count = hidden_in.shape[1]
    model_width = col_count * n_tp
    col_start = lax.axis_index("tp") * col_count
    heads_dev = state.shape[1]
    head_size = state.shape[2]
    top_count = routes.shape[1]
    local_experts = exp_gate.shape[0]
    expert_count = local_experts * n_ep
    capacity = max(2, 3 * seq_count * top_count // (2 * expert_count))
    slot_count = expert_count * capacity
    rows_full = lax.all_gather(hidden_in, "tp", axis=1, tiled=True)

    def project(weight):
        product = jnp.dot(rows_full, weight, preferred_element_type=jnp.float32)
        return rounded(product).reshape(seq_count, heads_dev, head_size)

    forget_pre = project(w_forget)
    forget = lower_bound + (1.0 - lower_bound) * jax.nn.sigmoid(forget_pre)
    key_part = (1.0 - lower_bound) * jax.nn.sigmoid(-forget_pre)
    values = project(w_input)
    queries = jax.nn.silu(project(w_query))
    out_gate = jax.nn.silu(project(w_outgate))
    new_state = forget[..., None] * state + key_part[..., None] * values[:, :, None, :]
    readout = jnp.einsum("bhd,bhdv->bhv", queries, new_state, precision=lax.Precision.HIGHEST)
    normed = readout * lax.rsqrt(jnp.mean(readout * readout, -1, keepdims=True) + EPS) * head_gain
    mixed = (normed * out_gate).astype(jnp.bfloat16).reshape(seq_count, heads_dev * head_size)
    branch = jnp.dot(mixed, w_out, preferred_element_type=jnp.float32)
    summed = lax.psum(branch.astype(jnp.bfloat16), "tp").astype(jnp.float32)
    residual = ALPHA * rows_full.astype(jnp.float32) + summed
    average = jnp.mean(residual, -1, keepdims=True)
    centered = residual - average
    variance = jnp.mean(centered * centered, -1, keepdims=True)
    normed_rows = (centered * lax.rsqrt(variance + EPS) * ln1_gain + ln1_bias).astype(jnp.bfloat16)
    routes_flat = routes.reshape(-1)
    one_hot = (routes_flat[:, None] == jnp.arange(expert_count, dtype=jnp.int32)[None, :]).astype(
        jnp.int32
    )
    position = jnp.sum((jnp.cumsum(one_hot, 0) - one_hot) * one_hot, 1)
    slot_index = routes_flat * capacity + position
    placing = (slot_index[:, None] == jnp.arange(slot_count, dtype=jnp.int32)[None, :]).astype(
        jnp.float32
    )
    chooser = jnp.sum(placing.reshape(seq_count, top_count, slot_count), 1).astype(jnp.bfloat16)
    weighted = jnp.sum(
        (placing * route_weights.reshape(-1)[:, None]).reshape(seq_count, top_count, slot_count), 1
    )
    own_cols = lax.dynamic_slice_in_dim(normed_rows, col_start, col_count, 1)
    picked = lax.dot_general(
        chooser, normed_rows, (((0,), (0,)), ((), ())), preferred_element_type=jnp.float32
    )
    arrived = lax.all_to_all(
        picked.astype(jnp.bfloat16).reshape(n_ep, local_experts * capacity, normed_rows.shape[1]),
        "ep",
        split_axis=0,
        concat_axis=0,
        tiled=True,
    )
    blocks = arrived.reshape(n_ep, local_experts, capacity, model_width)
    gate_part = jnp.einsum("gecd,edf->gecf", blocks, exp_gate, preferred_element_type=jnp.float32)
    up_part = jnp.einsum("gecd,edf->gecf", blocks, exp_up, preferred_element_type=jnp.float32)
    hidden_part = (jax.nn.silu(gate_part) * up_part).astype(jnp.bfloat16)
    expert_part = jnp.einsum(
        "gecf,efd->gecd", hidden_part, exp_down, preferred_element_type=jnp.float32
    )
    expert_part = expert_part.reshape(n_ep, local_experts * capacity, model_width).astype(
        jnp.bfloat16
    )
    shared_hidden = (
        jax.nn.silu(jnp.dot(normed_rows, sh_gate, preferred_element_type=jnp.float32))
        * jnp.dot(normed_rows, sh_up, preferred_element_type=jnp.float32)
    ).astype(jnp.bfloat16)
    shared_part = jnp.dot(shared_hidden, sh_down, preferred_element_type=jnp.float32)
    returned = lax.all_to_all(expert_part, "ep", split_axis=0, concat_axis=0, tiled=True)
    routed_partial = jnp.dot(
        weighted,
        returned.reshape(slot_count, model_width).astype(jnp.float32),
        precision=lax.Precision.HIGHEST,
    )
    combined = lax.psum_scatter(
        (routed_partial + shared_part).astype(jnp.bfloat16), "tp", scatter_dimension=1, tiled=True
    ).astype(jnp.float32)
    final_in = ALPHA * own_cols.astype(jnp.float32) + combined
    moments_two = lax.psum((jnp.sum(final_in, -1), jnp.sum(final_in * final_in, -1)), "tp")
    average_two = moments_two[0][:, None] / model_width
    variance_two = moments_two[1][:, None] / model_width - average_two * average_two
    gain_two = lax.dynamic_slice_in_dim(ln2_gain, col_start, col_count)
    bias_two = lax.dynamic_slice_in_dim(ln2_bias, col_start, col_count)
    mixed_out = (
        (final_in - average_two) * lax.rsqrt(variance_two + EPS) * gain_two + bias_two
    ).astype(jnp.bfloat16)
    return (mixed_out, new_state)


def solution(mesh):
    placed = (
        P("ep", "tp"),
        P("ep", "tp", None, None),
        P("tp", None),
        P(None, "tp"),
        P(None, "tp"),
        P(None, "tp"),
        P(None, "tp"),
        P(),
        P("tp", None),
        P(),
        P(),
        P("ep", None),
        P("ep", None),
        P("ep", None, "tp"),
        P("ep", None, "tp"),
        P("ep", "tp", None),
        P(None, "tp"),
        P(None, "tp"),
        P("tp", None),
        P(),
        P(),
    )
    return jax.shard_map(
        local,
        mesh=mesh,
        in_specs=placed,
        out_specs=(P("ep", "tp"), P("ep", "tp", None, None)),
        check_vma=False,
    )
```

profile of v0, /device:TPU:0, one launch (start us, length us, event | category | flops | bytes accessed | tf_op | source)
XLA Modules:
  0.0 155.0 jit_solution(1456552702936218920)
XLA Ops:
  7.2 0.0 copy-start
  7.2 0.9 copy.41
  8.1 0.1 eq.30
  8.2 0.1 fusion.39
  8.3 0.1 reduce_window_sum.11
  8.3 0.2 select_reduce_fusion.1
  8.5 0.1 reduce_sum.78
  8.6 0.8 copy.43
  9.4 10.7 %all_gather.3 = bf16[12,2048]{1,0:T(8,128)(2,1)S(1)} all-gather(bf16[12,256]{1,0:T(8,128)(2,1)} %param.21), channel_id=1, replica_groups=mesh['ep'=4,'tp'=8] {'tp'}, dimensions={1}, use_global_device_ids=true | all-gather | bytes 55296 | tf_op jit(solution)/shard_map/all_gather | solution.py:50
  20.1 2.0 %convolution_convert_fusion.2 = bf16[12,512]{1,0:T(8,128)(2,1)S(1)} fusion(bf16[12,2048]{1,0:T(8,128)(2,1)S(1)} %all_gather.3, bf16[2048,512]{1,0:T(8,128)(2,1)} %param.27), kind=kOutput, calls=%fused_computation.17 | convolution fusion | flops 25171968 | bytes 2158592 | tf_op jit(solution)/shard_map/dot_general | solution.py:53
  22.1 2.0 %convolution_convert_fusion.5 = bf16[12,512]{1,0:T(8,128)(2,1)S(1)} fusion(bf16[12,2048]{1,0:T(8,128)(2,1)S(1)} %all_gather.3, bf16[2048,512]{1,0:T(8,128)(2,1)} %param.26), kind=kOutput, calls=%fused_computation.20 | convolution fusion | flops 25171968 | bytes 2158592 | tf_op jit(solution)/shard_map/dot_general | solution.py:53
  24.1 2.0 %convolution_convert_fusion.3 = bf16[12,512]{1,0:T(8,128)(2,1)S(1)} fusion(bf16[12,2048]{1,0:T(8,128)(2,1)S(1)} %all_gather.3, bf16[2048,512]{1,0:T(8,128)(2,1)} %param.25), kind=kOutput, calls=%fused_computation.18 | convolution fusion | flops 25171968 | bytes 2158592 | tf_op jit(solution)/shard_map/dot_general | solution.py:53
  26.1 2.0 %convolution_convert_fusion.4 = bf16[12,512]{1,0:T(8,128)(2,1)S(1)} fusion(bf16[12,2048]{1,0:T(8,128)(2,1)S(1)} %all_gather.3, bf16[2048,512]{1,0:T(8,128)(2,1)} %param.24), kind=kOutput, calls=%fused_computation.19 | convolution fusion | flops 25171968 | bytes 2158592 | tf_op jit(solution)/shard_map/dot_general | solution.py:53
  28.3 3.8 %multiply_add_fusion = f32[12,4,128,128]{3,2,1,0:T(8,128)S(1)} fusion(f32[12,4,128,128]{3,2,1,0:T(8,128)} %param.22, f32[12,4,128]{2,1,0:T(4,128)S(1)} %reshape.140, f32[12,4,128]{2,1,0:T(4,128)S(1)} %bitcast.85, f32[12,4,128]{2,1,0:T(4,128)S(1)} %bitcast.84), kind=kLoop, calls=%fused_computation.6 | loop fusion | flops 2359296 | bytes 6365184 | tf_op jit(solution)/shard_map/add | solution.py:62
  32.1 0.0 copy-start.1
  32.1 0.0 copy-start.5
  32.1 1.6 %copy-done.1 = f32[12,4,128,128]{3,2,1,0:T(8,128)} copy-done((f32[12,4,128,128]{3,2,1,0:T(8,128)}, f32[12,4,128,128]{3,2,1,0:T(8,128)S(1)}, u32[]{:S(2)}) %copy-start.1) | copy-done | bytes 3145752
  33.7 2.8 %fusion.51 = f32[12,4,1,128]{3,2,1,0:T(1,128)S(1)} fusion(f32[12,4,128,1]{2,3,1,0:T(1,128)S(1)} %bitcast.83, f32[12,4,128,128]{3,2,1,0:T(8,128)S(1)} %multiply_add_fusion), kind=kOutput, calls=%fused_computation.69 | convolution fusion | flops 9437184 | bytes 3194880 | tf_op jit(solution)/shard_map/bhd,bhdv->bhv/dot_general | solution.py:63
  36.5 0.1 multiply_reduce_fusion.1
  36.6 0.1 fusion.40
  36.7 0.4 convolution_convert_fusion.1
  37.1 23.9 %psum.21 = bf16[12,2048]{1,0:T(8,128)(2,1)S(1)} all-reduce(bf16[12,2048]{1,0:T(8,128)(2,1)S(1)} %convolution_convert_fusion.1), channel_id=1, replica_groups=mesh['ep'=4,'tp'=8] {'tp'}, use_global_device_ids=true, to_apply=%region_1.2 | all-reduce | flops 24576 | bytes 98304 | tf_op jit(solution)/shard_map/psum | solution.py:67
  61.0 0.1 fusion.28
  61.1 0.2 multiply_reduce_fusion
  61.4 0.1 convert_reduce_fusion
  61.5 0.1 add_convert_fusion
  61.6 0.3 convolution_convert_fusion
  61.9 0.1 reshape.135
  62.0 13.9 %all_to_all.10 = bf16[4,18,2048]{2,1,0:T(8,128)(2,1)S(1)} all-to-all(bf16[4,18,2048]{2,1,0:T(8,128)(2,1)S(1)} %reshape.135), channel_id=1, replica_groups=mesh['ep'=4,'tp'=8] {'ep'}, dimensions={0} | all-to-all | bytes 589824 | tf_op jit(solution)/shard_map/all_to_all | solution.py:90
  75.8 0.2 copy.44
  76.0 2.9 %fusion.13 = f32[4,2,9,512]{3,2,0,1:T(8,128)S(1)} fusion(bf16[2,2048,512]{2,1,0:T(8,128)(2,1)} %param.34, bf16[4,2,9,2048]{3,0,2,1:T(4,128)(2,1)S(1)} %bitcast.78), kind=kOutput, calls=%fused_computation.13 | convolution fusion | flops 150994944 | bytes 4636672 | tf_op jit(solution)/shard_map/gecd,edf->gecf/dot_general | solution.py:98
  79.0 5.0 %fusion.9 = bf16[4,2,9,2048]{3,2,0,1:T(8,128)(2,1)S(1)} fusion(bf16[2,512,2048]{2,1,0:T(8,128)(2,1)} %param.36, bf16[2,2048,512]{2,1,0:T(8,128)(2,1)} %param.35, bf16[4,2,9,2048]{3,0,2,1:T(4,128)(2,1)S(1)} %bitcast.79, f32[4,2,9,512]{3,2,0,1:T(8,128)S(1)} %fusion.13), kind=kOutput, calls=%fused_computation.8 | convolution fusion | flops 302358528 | bytes 9125888 | tf_op jit(solution)/shard_map/gecf,efd->gecd/dot_general | solution.py:101
  84.0 0.2 copy.47
  84.2 0.9 copy.48
  85.2 3.5 %all-to-all-start.1 = ((bf16[4,18,2048]{2,1,0:T(8,128)(2,1)}), bf16[4,18,2048]{2,1,0:T(8,128)(2,1)S(1)}, u32[]{:S(2)}, u32[]{:S(2)}) async-start(bf16[4,18,2048]{2,1,0:T(8,128)(2,1)} %copy.48), calls=%async_computation.1 | async-start | bytes 786432 | tf_op jit(solution)/shard_map/all_to_all | solution.py:112
  88.6 0.0 reduce-scatter.2.cloned.1.call-start
  88.7 1.1 fusion.53
  89.8 8.4 %all-to-all-done.1 = bf16[4,18,2048]{2,1,0:T(8,128)(2,1)S(1)} async-done(((bf16[4,18,2048]{2,1,0:T(8,128)(2,1)}), bf16[4,18,2048]{2,1,0:T(8,128)(2,1)S(1)}, u32[]{:S(2)}, u32[]{:S(2)}) %all-to-all-start.1) | async-done | bytes 294944 | tf_op jit(solution)/shard_map/all_to_all | solution.py:112
  98.2 0.1 reshape.137
  98.2 0.3 fusion.52
  98.5 2.0 %fusion.12 = bf16[12,2048]{1,0:T(8,128)(2,1)} fusion(f32[12,2048]{1,0:T(8,128)S(1)} %fusion.52, bf16[64,2048]{1,0:T(8,128)(2,1)S(1)} %copy-done.2, bf16[12,2048]{1,0:T(8,128)(2,1)S(1)} %add_convert_fusion, bf16[2048,64]{0,1:T(8,128)(2,1)} %param.38, f32[12,64]{1,0:T(8,128)S(1)} %fusion.53), kind=kOutput, calls=%fused_computation.11 | convolution fusion | flops 6345216 | bytes 723968 | tf_op jit(solution)/shard_map/dot_general | solution.py:111
  100.5 0.0 reduce-scatter.2.cloned.1.call-update
  100.5 0.8 dynamic_slice.11
  101.3 0.8 dynamic_slice.10
  102.0 31.7 %reduce-scatter.2.cloned.1.call-done = bf16[12,256]{1,0:T(8,128)(2,1)} async-done(((bf16[12,2048]{1,0:T(8,128)(2,1)}), bf16[12,256]{1,0:T(8,128)(2,1)}) %reduce-scatter.2.cloned.1.call-update) | async-done | bytes 6160 | tf_op jit(solution)/shard_map/reduce_scatter | solution.py:118
  133.8 0.8 fusion.41
  134.6 12.2 %all-reduce = (f32[12]{0:T(128)S(1)}, f32[12]{0:T(128)S(1)}) all-reduce(f32[12]{0:T(128)S(1)} %get-tuple-element.3, f32[12]{0:T(128)S(1)} %get-tuple-element.2), channel_id=1, replica_groups=mesh['ep'=4,'tp'=8] {'tp'}, use_global_device_ids=true, to_apply=%region_12.13 | all-reduce | flops 24 | bytes 192 | tf_op jit(solution)/shard_map/psum | solution.py:122
  146.8 1.4 add_convert_fusion.1
  (28 shorter events, 0.3 us)
Async XLA Ops:
  7.2 29.6 %copy-start = (bf16[512,2048]{1,0:T(8,128)(2,1)S(1)}, bf16[512,2048]{1,0:T(8,128)(2,1)}, u32[]{:S(2)}) copy-start(bf16[512,2048]{1,0:T(8,128)(2,1)} %param.29) | copy-start | bytes 6291460
  22.1 6.1 %copy-start.3 = (f32[4,128]{1,0:T(4,128)S(1)}, f32[4,128]{1,0:T(4,128)}, u32[]{:S(2)}) copy-start(f32[4,128]{1,0:T(4,128)} %param.23) | copy-start | bytes 6148
  32.1 1.7 %copy-start.1 = (f32[12,4,128,128]{3,2,1,0:T(8,128)}, f32[12,4,128,128]{3,2,1,0:T(8,128)S(1)}, u32[]{:S(2)}) copy-start(f32[12,4,128,128]{3,2,1,0:T(8,128)S(1)} %multiply_add_fusion) | copy-start | bytes 9437188
  32.1 4.5 %copy-start.6 = (f32[128]{0:T(128)S(1)}, f32[128]{0:T(128)}, u32[]{:S(2)}) copy-start(f32[128]{0:T(128)} %param.28) | copy-start | bytes 1540
  32.1 29.4 %copy-start.4 = (f32[2048]{0:T(1024)S(1)}, f32[2048]{0:T(1024)}, u32[]{:S(2)}) copy-start(f32[2048]{0:T(1024)} %param.31) | copy-start | bytes 24580
  32.1 29.4 %copy-start.5 = (f32[2048]{0:T(1024)S(1)}, f32[2048]{0:T(1024)}, u32[]{:S(2)}) copy-start(f32[2048]{0:T(1024)} %param.30) | copy-start | bytes 24580
  84.0 14.5 %copy-start.2 = (bf16[64,2048]{1,0:T(8,128)(2,1)S(1)}, bf16[64,2048]{1,0:T(8,128)(2,1)}, u32[]{:S(2)}) copy-start(bf16[64,2048]{1,0:T(8,128)(2,1)} %param.39) | copy-start | bytes 786436
  85.2 13.0 %all-to-all-start.1 = ((bf16[4,18,2048]{2,1,0:T(8,128)(2,1)}), bf16[4,18,2048]{2,1,0:T(8,128)(2,1)S(1)}, u32[]{:S(2)}, u32[]{:S(2)}) async-start(bf16[4,18,2048]{2,1,0:T(8,128)(2,1)} %copy.48), calls=%async_computation.1 | async-start | bytes 786432 | tf_op jit(solution)/shard_map/all_to_all | solution.py:112
  88.6 45.2 %reduce-scatter.2.cloned.1.call-start = ((), (), s32[]{:S(2)}) async-start(), calls=%async_computation.3 | async-start | bytes 73728 | tf_op jit(solution)/shard_map/reduce_scatter | solution.py:118
Sparse Core Ops, SparseCore 0:
  100.6 33.1 reduce-scatter.1
where the time goes:
time: 156 us; the launch traced here: 155 us
  blocking collectives  60.6 us (39%)
  waiting for transfers between devices  40.1 us (26%)
  matrix products  22.5 us (14%)
  between operations  14.3 us (9%)
  other arithmetic  7.16 us (5%)
  local copies, waits for them, and re-layouts  6.75 us (4%)
  starting transfers between devices  3.5 us (2%)
    reduce_scatter x1, waiting for transfers between devices, local(): lax.psum_scatter((routed_partial + shared_part).astype(jnp.bfloat16), 'tp...  31.7 us
    psum x1, blocking collectives, local(): summed = lax.psum(branch.astype(jnp.bfloat16), 'tp').astype(jnp.float32)  23.9 us
    all_to_all x1, blocking collectives, local(): lax.all_to_all(picked.astype(jnp.bfloat16).reshape(n_ep, local_experts *...  13.9 us
    psum x1, blocking collectives, local(): lax.psum((jnp.sum(final_in, -1), jnp.sum(final_in * final_in, -1)), 'tp')  12.2 us
    all_gather x1, blocking collectives, local(): rows_full = lax.all_gather(hidden_in, 'tp', axis=1, tiled=True)  10.7 us
    all_to_all x1, waiting for transfers between devices, local(): lax.all_to_all(expert_part, 'ep', split_axis=0, concat_axis=0, tiled=True)  8.36 us
    dot_general x4, matrix products, project(): product = jnp.dot(rows_full, weight, preferred_element_type=jnp.float32)  7.85 us
    dot_general x1, matrix products, local(): jnp.einsum('gecf,efd->gecd', hidden_part, exp_down, preferred_element_typ...  4.99 us
  transfers between devices with their start and end apart: 2, of which 2 were waited for; matrix products, arithmetic and copies ran while one was open for 2% of the time, Pallas kernels for 0%

commit v1 on v0

--- a/solution.py
+++ b/solution.py
@@ -1,10 +1,395 @@
+import functools
+
 import jax
 import jax.numpy as jnp
 from jax import lax
+from jax.experimental import pallas as pl
+from jax.experimental.pallas import tpu as pltpu
 from jax.sharding import PartitionSpec as P
 
 EPS = 1e-05
 ALPHA = 2.0**0.25
+MESH = pl.DeviceIdType.MESH
+F32 = jnp.float32
+BF16 = jnp.bfloat16
+
+
+def sigmoid(value):
+    return jax.nn.sigmoid(value)
+
+
+def silu(value):
+    return value * jax.nn.sigmoid(value)
+
+
+def dot(left, right):
+    return jnp.dot(left, right, preferred_element_type=F32)
+
+
+def layer_kernel(
+    n_ep,
+    n_tp,
+    hid,
+    lb,
+    hg,
+    g1,
+    b1,
+    routes,
+    rw,
+    g2,
+    b2,
+    state_h,
+    wf_h,
+    wi_h,
+    wq_h,
+    wo_h,
+    wout_h,
+    eg_h,
+    eu_h,
+    ed_h,
+    sg_h,
+    su_h,
+    sd_h,
+    out,
+    ns_h,
+    st,
+    wf,
+    wi,
+    wq,
+    wo,
+    wout,
+    eg,
+    eu,
+    ed,
+    sg,
+    su,
+    sd,
+    xf,
+    xs,
+    cws,
+    cols_t,
+    vals,
+    ro,
+    rs_send,
+    rs,
+    res,
+    nr,
+    cw_col,
+    a2a_send,
+    a2a,
+    stat,
+    load_sem,
+    ns_sem,
+    send_sem,
+    recv_sem,
+):
+    n_all = n_ep * n_tp
+    me_e = lax.axis_index("ep")
+    me_t = lax.axis_index("tp")
+    me = me_e * n_tp + me_t
+    seqs = hid.shape[0]
+    cols = hid.shape[1]
+    rows = xf.shape[0]
+    heads = lb.shape[0]
+    head = lb.shape[1]
+    local_experts = eg.shape[0]
+
+    def device(index):
+        return (index // n_tp, lax.rem(index, n_tp))
+
+    first = [(wf_h, wf), (wi_h, wi), (wq_h, wq), (wo_h, wo), (state_h, st), (wout_h, wout)]
+    second = [(eg_h, eg), (eu_h, eu), (sg_h, sg), (su_h, su), (ed_h, ed), (sd_h, sd)]
+    loads = {}
+
+    def start_loads(pairs, base):
+        for i, (src, dst) in enumerate(pairs):
+            loads[base + i] = pltpu.make_async_copy(src, dst, load_sem.at[base + i])
+            loads[base + i].start()
+
+    barrier = pltpu.get_barrier_semaphore()
+    for k in range(1, n_all):
+        pl.semaphore_signal(
+            barrier, inc=1, device_id=device(lax.rem(me + k, n_all)), device_id_type=MESH
+        )
+    start_loads(first, 0)
+
+    xf[...] = jnp.zeros_like(xf)
+    xf[0:seqs, :] = hid[...].astype(F32)
+    own_hidden = xf[...]
+    xs[me_t] = own_hidden.astype(BF16)
+    lanes = lax.broadcasted_iota(jnp.int32, (seqs, cws.shape[2]), 1)
+    own_cw = jnp.zeros(lanes.shape, F32)
+    for k in range(routes.shape[1]):
+        own_cw += jnp.where(lanes == routes[:, k : k + 1], rw[:, k : k + 1], 0.0)
+    cws[me_e] = jnp.zeros(cws.shape[1:], F32)
+    cws[me_e, 0:seqs, :] = own_cw
+
+    pl.semaphore_wait(barrier, n_all - 1)
+
+    sends = []
+
+    def send(src, dst, phase, target):
+        copy = pltpu.make_async_remote_copy(
+            src_ref=src,
+            dst_ref=dst,
+            send_sem=send_sem.at[phase],
+            recv_sem=recv_sem.at[phase],
+            device_id=target,
+            device_id_type=MESH,
+        )
+        copy.start()
+        sends.append(copy)
+
+    def arrived(buffer, count, phase):
+        part = buffer.at[pl.ds(0, count)]
+        pltpu.make_async_copy(part, part, recv_sem.at[phase]).wait()
+
+    for k in range(1, n_tp):
+        send(xs.at[me_t], xs.at[me_t], 0, (me_e, lax.rem(me_t + k, n_tp)))
+    for k in range(1, n_ep):
+        send(cws.at[me_e], cws.at[me_e], 1, (lax.rem(me_e + k, n_ep), me_t))
+    start_loads(second, len(first))
+
+    arrived(xs, n_tp - 1, 0)
+    x_full = jnp.concatenate([xs[t] for t in range(n_tp)], axis=1)
+
+    def project(weight, index):
+        loads[index].wait()
+        return dot(x_full, weight[...]).astype(BF16).astype(F32)
+
+    forget_pre = project(wf, 0)
+    value_in = project(wi, 1)
+    query = silu(project(wq, 2))
+    out_gate = silu(project(wo, 3))
+    for h in range(heads):
+        span = slice(h * head, (h + 1) * head)
+        bound = lb[h : h + 1, :]
+        pre = forget_pre[:, span]
+        forget = bound + (1.0 - bound) * sigmoid(pre)
+        key = (1.0 - bound) * sigmoid(-pre)
+        stacked = jnp.concatenate(
+            [forget, key, query[:, span], jnp.zeros((head - 3 * rows, head), F32)], axis=0
+        )
+        cols_t[h] = stacked.T
+        vals[h] = value_in[:, span]
+    loads[4].wait()
+    ro[...] = jnp.zeros_like(ro)
+    outs = []
+    for h in range(heads):
+        for b in range(seqs):
+            f_col = cols_t[h, :, b : b + 1]
+            k_col = cols_t[h, :, rows + b : rows + b + 1]
+            q_col = cols_t[h, :, 2 * rows + b : 2 * rows + b + 1]
+            new = f_col * st[b, h] + k_col * vals[h, b : b + 1, :]
+            st[b, h] = new
+            ro[h, b : b + 1, :] = jnp.sum(q_col * new, axis=0, keepdims=True)
+        outs.append(pltpu.make_async_copy(st.at[:, h], ns_h.at[:, h], ns_sem.at[h]))
+        outs[-1].start()
+    mixed = []
+    for h in range(heads):
+        readout = ro[h]
+        scale = lax.rsqrt(jnp.mean(readout * readout, -1, keepdims=True) + EPS)
+        gate = out_gate[:, h * head : (h + 1) * head]
+        mixed.append((readout * scale * hg[...] * gate).astype(BF16))
+    mixed = jnp.concatenate(mixed, axis=1)
+    loads[5].wait()
+    for t in range(n_tp):
+        block = dot(mixed, wout[:, t * cols : (t + 1) * cols])
+        rs_send[t] = block.astype(BF16)
+    for k in range(1, n_tp):
+        peer = lax.rem(me_t + k, n_tp)
+        send(rs_send.at[peer], rs.at[me_t], 2, (me_e, peer))
+    rs[me_t] = rs_send[me_t]
+    arrived(rs, n_tp - 1, 2)
+    total = ALPHA * own_hidden
+    for t in range(n_tp):
+        total += rs[t].astype(F32)
+    res[me] = total.astype(BF16)
+    for k in range(1, n_all):
+        send(res.at[me], res.at[me], 3, device(lax.rem(me + k, n_all)))
+    arrived(cws, n_ep - 1, 1)
+    for g in range(n_ep):
+        for j in range(local_experts):
+            at = lax.broadcasted_iota(jnp.int32, cws.shape[1:], 1)
+            cw_col[j, g * rows : (g + 1) * rows, :] = jnp.sum(
+                jnp.where(at == me_e * local_experts + j, cws[g], 0.0), axis=1, keepdims=True
+            )
+    arrived(res, n_all - 1, 3)
+    width = n_tp * cols
+    for g in range(n_ep):
+        row = jnp.concatenate([res[g * n_tp + t] for t in range(n_tp)], axis=1).astype(F32)
+        centered = row - jnp.sum(row, -1, keepdims=True) / width
+        variance = jnp.sum(centered * centered, -1, keepdims=True) / width
+        normed = centered * lax.rsqrt(variance + EPS) * g1[...] + b1[...]
+        nr[g * rows : (g + 1) * rows, :] = normed.astype(BF16)
+    all_rows = nr[...]
+    base = len(first)
+    loads[base].wait()
+    loads[base + 1].wait()
+    hidden = []
+    for j in range(local_experts):
+        hidden.append((silu(dot(all_rows, eg[j])) * dot(all_rows, eu[j])).astype(BF16))
+    loads[base + 2].wait()
+    loads[base + 3].wait()
+    own_rows = nr[pl.ds(pl.multiple_of(me_e * rows, rows), rows), :]
+    shared = (silu(dot(own_rows, sg[...])) * dot(own_rows, su[...])).astype(BF16)
+    loads[base + 4].wait()
+    loads[base + 5].wait()
+    weights = [cw_col[j] for j in range(local_experts)]
+    for t in range(n_tp):
+        span = slice(t * cols, (t + 1) * cols)
+        acc = jnp.zeros((n_ep * rows, cols), F32)
+        for j in range(local_experts):
+            part = dot(hidden[j], ed[j, :, span]).astype(BF16).astype(F32)
+            acc += weights[j] * part
+        shared_part = dot(shared, sd[:, span])
+        for g in range(n_ep):
+            mine = jnp.where(me_e == g, 1.0, 0.0)
+            block = acc[g * rows : (g + 1) * rows] + mine * shared_part
+            a2a_send[g * n_tp + t] = block.astype(BF16)
+    for k in range(1, n_all):
+        peer = lax.rem(me + k, n_all)
+        send(a2a_send.at[peer], a2a.at[me], 4, device(peer))
+    a2a[me] = a2a_send[me]
+    start = pl.multiple_of(me_t * cols, cols)
+    own_cols = nr[pl.ds(pl.multiple_of(me_e * rows, rows), rows), pl.ds(start, cols)]
+    final = ALPHA * own_cols.astype(F32)
+    arrived(a2a, n_all - 1, 4)
+    for i in range(n_all):
+        final += a2a[i].astype(F32)
+    mean_own = jnp.sum(final, -1, keepdims=True) / cols
+    apart = final - mean_own
+    spread_own = jnp.sum(apart * apart, -1, keepdims=True)
+    lane = lax.broadcasted_iota(jnp.int32, stat.shape[1:], 1)
+    stat[me_t] = jnp.where(lane == 0, mean_own, spread_own)
+    for k in range(1, n_tp):
+        send(stat.at[me_t], stat.at[me_t], 5, (me_e, lax.rem(me_t + k, n_tp)))
+    gain = g2[:, pl.ds(start, cols)]
+    bias = b2[:, pl.ds(start, cols)]
+    arrived(stat, n_tp - 1, 5)
+    means = [stat[t, :, 0:1] for t in range(n_tp)]
+    mean = sum(means) / n_tp
+    spread = jnp.zeros_like(mean)
+    for t in range(n_tp):
+        spread += stat[t, :, 1:2] + cols * (means[t] - mean) * (means[t] - mean)
+    result = (final - mean) * lax.rsqrt(spread / width + EPS) * gain + bias
+    out[...] = result[0:seqs, :].astype(BF16)
+    for copy in sends:
+        copy.wait_send()
+    for copy in outs:
+        copy.wait()
+
+
+def fused(
+    hidden_in,
+    state,
+    lower_bound,
+    w_forget,
+    w_input,
+    w_query,
+    w_outgate,
+    head_gain,
+    w_out,
+    ln1_gain,
+    ln1_bias,
+    routes,
+    route_weights,
+    exp_gate,
+    exp_up,
+    exp_down,
+    sh_gate,
+    sh_up,
+    sh_down,
+    ln2_gain,
+    ln2_bias,
+):
+    n_tp = lax.axis_size("tp")
+    n_ep = lax.axis_size("ep")
+    n_all = n_tp * n_ep
+    seqs, cols = hidden_in.shape
+    rows = -(-seqs // 16) * 16
+    heads, head = lower_bound.shape
+    local_experts = exp_gate.shape[0]
+    whole = [
+        state,
+        w_forget,
+        w_input,
+        w_query,
+        w_outgate,
+        w_out,
+        exp_gate,
+        exp_up,
+        exp_down,
+        sh_gate,
+        sh_up,
+        sh_down,
+    ]
+    vmem = pl.BlockSpec(memory_space=pltpu.VMEM)
+    hbm = pl.BlockSpec(memory_space=pltpu.HBM)
+    scratch = [pltpu.VMEM(a.shape, a.dtype) for a in whole]
+    scratch += [
+        pltpu.VMEM((rows, cols), F32),
+        pltpu.VMEM((n_tp, rows, cols), BF16),
+        pltpu.VMEM((n_ep, rows, 128), F32),
+        pltpu.VMEM((heads, head, head), F32),
+        pltpu.VMEM((heads, rows, head), F32),
+        pltpu.VMEM((heads, rows, head), F32),
+        pltpu.VMEM((n_tp, rows, cols), BF16),
+        pltpu.VMEM((n_tp, rows, cols), BF16),
+        pltpu.VMEM((n_all, rows, cols), BF16),
+        pltpu.VMEM((n_ep * rows, n_tp * cols), BF16),
+        pltpu.VMEM((local_experts, n_ep * rows, 1), F32),
+        pltpu.VMEM((n_all, rows, cols), BF16),
+        pltpu.VMEM((n_all, rows, cols), BF16),
+        pltpu.VMEM((n_tp, rows, 128), F32),
+        pltpu.SemaphoreType.DMA((12,)),
+        pltpu.SemaphoreType.DMA((heads,)),
+        pltpu.SemaphoreType.DMA((6,)),
+        pltpu.SemaphoreType.DMA((6,)),
+    ]
+    kernel = functools.partial(layer_kernel, n_ep, n_tp)
+    row = lambda a: a.reshape(1, -1)
+    mixed_out, new_state = pl.pallas_call(
+        kernel,
+        out_shape=(
+            jax.ShapeDtypeStruct(hidden_in.shape, BF16),
+            jax.ShapeDtypeStruct(state.shape, F32),
+        ),
+        in_specs=[vmem] * 9 + [hbm] * 12,
+        out_specs=(vmem, hbm),
+        scratch_shapes=scratch,
+        compiler_params=pltpu.CompilerParams(
+            collective_id=0, has_side_effects=True, vmem_limit_bytes=60 * 1024 * 1024
+        ),
+    )(
+        hidden_in,
+        lower_bound,
+        row(head_gain),
+        row(ln1_gain),
+        row(ln1_bias),
+        routes,
+        route_weights,
+        row(ln2_gain),
+        row(ln2_bias),
+        *whole,
+    )
+    return (mixed_out, new_state)
+
+
+def fits(mesh, hidden_in, state, exp_gate):
+    n_tp = mesh.shape["tp"]
+    n_ep = mesh.shape["ep"]
+    seqs = hidden_in.shape[0] // n_ep
+    cols = hidden_in.shape[1] // n_tp
+    weights = 3 * exp_gate.size * 2 // (n_tp * n_ep) + state.size * 4 // (n_tp * n_ep)
+    return (
+        cols % 128 == 0
+        and seqs <= 16
+        and state.shape[2] == 128
+        and exp_gate.shape[0] <= 128
+        and n_tp * n_ep <= 64
+        and weights <= 24 * 1024 * 1024
+    )
 
 
 def rounded(value):
@@ -154,10 +539,15 @@
         P(),
         P(),
     )
-    return jax.shard_map(
-        local,
-        mesh=mesh,
-        in_specs=placed,
-        out_specs=(P("ep", "tp"), P("ep", "tp", None, None)),
-        check_vma=False,
-    )
+
+    def layer(*arrays):
+        chosen = fused if fits(mesh, arrays[0], arrays[1], arrays[13]) else local
+        return jax.shard_map(
+            chosen,
+            mesh=mesh,
+            in_specs=placed,
+            out_specs=(P("ep", "tp"), P("ep", "tp", None, None)),
+            check_vma=False,
+        )(*arrays)
+
+    return layer

time: 156 us -> 52.3 us (0.34)
  blocking collectives: 60.6 us -> 0 us
  waiting for transfers between devices: 40.1 us -> 0 us
  Pallas kernels: 0 us -> 39.5 us
  matrix products: 22.5 us -> 0 us
  between operations: 14.3 us -> 0.64 us
  other arithmetic: 7.16 us -> 0 us
  local copies, waits for them, and re-layouts: 6.75 us -> 11.8 us
  starting transfers between devices: 3.5 us -> 0 us
    pallas_call x0 -> x1, Pallas kernels: none -> 39.5 us  [fused(): pl.pallas_call(kernel, out_shape=(jax.ShapeDtypeStruct(hidden_in.shape, B...]
    psum x2 -> x0, blocking collectives: 36 us -> none  [the longest x1 23.9 us: local(): summed = lax.psum(branch.astype(jnp.bfloat16), 'tp').astype(jnp.float32)]
    reduce_scatter x1 -> x0, waiting for transfers between devices: 31.7 us -> none  [local(): lax.psum_scatter((routed_partial + shared_part).astype(jnp.bfloat16), 'tp...]
    dot_general x12 -> x0, matrix products: 22.5 us -> none  [the longest x4 7.85 us: project(): product = jnp.dot(rows_full, weight, preferred_element_type=jnp.float32)]
    all_to_all x1 -> x0, blocking collectives: 13.9 us -> none  [local(): lax.all_to_all(picked.astype(jnp.bfloat16).reshape(n_ep, local_experts *...]
    all_gather x1 -> x0, blocking collectives: 10.7 us -> none  [local(): rows_full = lax.all_gather(hidden_in, 'tp', axis=1, tiled=True)]
    unnamed x20 -> x6, local copies, waits for them, and re-layouts: 3.39 us -> 11.8 us
    all_to_all x1 -> x0, waiting for transfers between devices: 8.36 us -> none  [local(): lax.all_to_all(expert_part, 'ep', split_axis=0, concat_axis=0, tiled=True)]
  transfers between devices with their start and end apart: 2 -> 0, of which waited for: 2 -> 0; matrix products, arithmetic and copies ran while one was open for 2% -> 0% of each run, Pallas kernels for 0% -> 0%
where the time goes in v1:
time: 52.3 us; the launch traced here: 52 us
  Pallas kernels  39.5 us (76%)
  local copies, waits for them, and re-layouts  11.8 us (23%)
  between operations  0.64 us (1%)
    pallas_call x1, Pallas kernels, fused(): pl.pallas_call(kernel, out_shape=(jax.ShapeDtypeStruct(hidden_in.shape, B...  39.5 us
    unnamed x6, local copies, waits for them, and re-layouts  11.8 us

profile of v1, /device:TPU:0, one launch (start us, length us, event | category | flops | bytes accessed | tf_op | source)
XLA Modules:
  0.0 52.0 jit_solution(6810234190871944260)
XLA Ops:
  0.6 1.4 %copy.23.routes = s32[12,4]{1,0:T(8,128)} copy(s32[12,4]{0,1:T(4,128)} %param.32) | data formatting | bytes 384 | tf_op args[11]
  2.0 1.4 %copy.24.rw = f32[12,4]{1,0:T(8,128)} copy(f32[12,4]{0,1:T(4,128)} %param.33) | data formatting | bytes 384 | tf_op args[12]
  3.3 2.0 %copy.25.sg_h = bf16[2048,64]{1,0:T(8,128)(2,1)} copy(bf16[2048,64]{0,1:T(8,128)(2,1)} %param.37) | data formatting | bytes 524288 | tf_op args[16]
  5.3 1.9 %copy.26.su_h = bf16[2048,64]{1,0:T(8,128)(2,1)} copy(bf16[2048,64]{0,1:T(8,128)(2,1)} %param.38) | data formatting | bytes 524288 | tf_op args[17]
  7.2 39.5 %shard_map.212 = (bf16[12,256]{1,0:T(8,128)(2,1)}, f32[12,4,128,128]{3,2,1,0:T(8,128)}) custom-call(bf16[12,256]{1,0:T(8,128)(2,1)} %hid.1, f32[4,128]{1,0:T(4,128)} %lb.1, f32[1,128]{1,0:T(1,128)} %bitcast.9, f32[1,2048]{1,0:T(1,128)} %bitcast.5, f32[1,2048]{1,0:T(1,128)} %bitcast.6, s32[12,4]{1,0:T(8,128)} %copy.23.routes, f32[12,4]{1,0:T(8,128)} %copy.24.rw, ...), custom_call_target="tpu_custom_call" | custom-call | tf_op jit(solution)/shard_map/pallas_call | solution.py:352
  46.8 1.3 %copy.29 = bf16[12,256]{1,0:T(8,128)(2,1)} copy(bf16[12,256]{1,0:T(8,128)(2,1)} %get-tuple-element.4) | data formatting | bytes 12288
  48.1 3.9 %copy.30 = f32[12,4,128,128]{3,2,1,0:T(8,128)} copy(f32[12,4,128,128]{3,2,1,0:T(8,128)} %get-tuple-element.5) | data formatting | bytes 6291456

commit v2 on v1

--- a/solution.py
+++ b/solution.py
@@ -24,6 +24,11 @@
 
 def dot(left, right):
     return jnp.dot(left, right, preferred_element_type=F32)
+
+
+def dot_t(left, right):
+    dims = (((1,), (1,)), ((), ()))
+    return lax.dot_general(left, right, dims, preferred_element_type=F32)
 
 
 def layer_kernel(
@@ -77,16 +82,18 @@
     cw_col,
     a2a_send,
     a2a,
+    z_send,
+    z_recv,
+    acc_buf,
+    cw_t,
     stat,
     load_sem,
     ns_sem,
     send_sem,
     recv_sem,
 ):
-    n_all = n_ep * n_tp
     me_e = lax.axis_index("ep")
     me_t = lax.axis_index("tp")
-    me = me_e * n_tp + me_t
     seqs = hid.shape[0]
     cols = hid.shape[1]
     rows = xf.shape[0]
@@ -94,9 +101,6 @@
     head = lb.shape[1]
     local_experts = eg.shape[0]
 
-    def device(index):
-        return (index // n_tp, lax.rem(index, n_tp))
-
     first = [(wf_h, wf), (wi_h, wi), (wq_h, wq), (wo_h, wo), (state_h, st), (wout_h, wout)]
     second = [(eg_h, eg), (eu_h, eu), (sg_h, sg), (su_h, su), (ed_h, ed), (sd_h, sd)]
     loads = {}
@@ -107,24 +111,27 @@
             loads[base + i].start()
 
     barrier = pltpu.get_barrier_semaphore()
-    for k in range(1, n_all):
-        pl.semaphore_signal(
-            barrier, inc=1, device_id=device(lax.rem(me + k, n_all)), device_id_type=MESH
-        )
+    for k in range(1, n_ep):
+        target = (lax.rem(me_e + k, n_ep), me_t)
+        pl.semaphore_signal(barrier, inc=1, device_id=target, device_id_type=MESH)
+    for k in range(1, n_tp):
+        target = (me_e, lax.rem(me_t + k, n_tp))
+        pl.semaphore_signal(barrier, inc=1, device_id=target, device_id_type=MESH)
     start_loads(first, 0)
 
     xf[...] = jnp.zeros_like(xf)
     xf[0:seqs, :] = hid[...].astype(F32)
     own_hidden = xf[...]
     xs[me_t] = own_hidden.astype(BF16)
-    lanes = lax.broadcasted_iota(jnp.int32, (seqs, cws.shape[2]), 1)
-    own_cw = jnp.zeros(lanes.shape, F32)
-    for k in range(routes.shape[1]):
-        own_cw += jnp.where(lanes == routes[:, k : k + 1], rw[:, k : k + 1], 0.0)
-    cws[me_e] = jnp.zeros(cws.shape[1:], F32)
-    cws[me_e, 0:seqs, :] = own_cw
-
-    pl.semaphore_wait(barrier, n_all - 1)
+    names = lax.broadcasted_iota(jnp.int32, (cw_t.shape[0], seqs), 0)
+    own_cw = jnp.zeros(names.shape, F32)
+    for k in range(routes.shape[0]):
+        own_cw += jnp.where(names == routes[k : k + 1, :], rw[k : k + 1, :], 0.0)
+    cw_t[...] = jnp.zeros_like(cw_t)
+    cw_t[:, 0:seqs] = own_cw
+    cws[me_e] = cw_t[...].T[0:rows, :]
+
+    pl.semaphore_wait(barrier, n_ep + n_tp - 2)
 
     sends = []
 
@@ -193,20 +200,43 @@
         mixed.append((readout * scale * hg[...] * gate).astype(BF16))
     mixed = jnp.concatenate(mixed, axis=1)
     loads[5].wait()
-    for t in range(n_tp):
-        block = dot(mixed, wout[:, t * cols : (t + 1) * cols])
-        rs_send[t] = block.astype(BF16)
-    for k in range(1, n_tp):
+    for k in list(range(1, n_tp)) + [0]:
         peer = lax.rem(me_t + k, n_tp)
-        send(rs_send.at[peer], rs.at[me_t], 2, (me_e, peer))
-    rs[me_t] = rs_send[me_t]
+        block = dot(mixed, wout[:, pl.ds(pl.multiple_of(peer * cols, cols), cols)])
+        if k:
+            rs_send[peer] = block.astype(BF16)
+            send(rs_send.at[peer], rs.at[me_t], 2, (me_e, peer))
+        else:
+            rs[me_t] = block.astype(BF16)
     arrived(rs, n_tp - 1, 2)
     total = ALPHA * own_hidden
     for t in range(n_tp):
         total += rs[t].astype(F32)
-    res[me] = total.astype(BF16)
-    for k in range(1, n_all):
-        send(res.at[me], res.at[me], 3, device(lax.rem(me + k, n_all)))
+    res[me_e, me_t] = total.astype(BF16)
+    near = sorted(range(n_ep), key=lambda k: min(k, n_ep - k))
+    for k in reversed(near[1:]):
+        piece = res.at[me_e, me_t]
+        send(piece, piece, 5 + k, (lax.rem(me_e + k, n_ep), me_t))
+    width = n_tp * cols
+
+    def forward(k):
+        group = lax.rem(me_e + n_ep - k, n_ep)
+        piece = res.at[group, me_t]
+        if k:
+            pltpu.make_async_copy(piece, piece, recv_sem.at[5 + k]).wait()
+        for i in range(1, n_tp):
+            send(piece, piece, 5 + n_ep + k, (me_e, lax.rem(me_t + i, n_tp)))
+
+    def norm_group(k):
+        group = lax.rem(me_e + n_ep - k, n_ep)
+        arrived(res.at[group], n_tp - 1, 5 + n_ep + k)
+        row = jnp.concatenate([res[group, t] for t in range(n_tp)], axis=1).astype(F32)
+        centered = row - jnp.sum(row, -1, keepdims=True) / width
+        variance = jnp.sum(centered * centered, -1, keepdims=True) / width
+        normed = centered * lax.rsqrt(variance + EPS) * g1[...] + b1[...]
+        nr[pl.ds(pl.multiple_of(group * rows, rows), rows), :] = normed.astype(BF16)
+
+    forward(0)
     arrived(cws, n_ep - 1, 1)
     for g in range(n_ep):
         for j in range(local_experts):
@@ -214,49 +244,57 @@
             cw_col[j, g * rows : (g + 1) * rows, :] = jnp.sum(
                 jnp.where(at == me_e * local_experts + j, cws[g], 0.0), axis=1, keepdims=True
             )
-    arrived(res, n_all - 1, 3)
-    width = n_tp * cols
-    for g in range(n_ep):
-        row = jnp.concatenate([res[g * n_tp + t] for t in range(n_tp)], axis=1).astype(F32)
-        centered = row - jnp.sum(row, -1, keepdims=True) / width
-        variance = jnp.sum(centered * centered, -1, keepdims=True) / width
-        normed = centered * lax.rsqrt(variance + EPS) * g1[...] + b1[...]
-        nr[g * rows : (g + 1) * rows, :] = normed.astype(BF16)
+    base = len(first)
+    for k in near[1:]:
+        forward(k)
+    norm_group(0)
+    own_rows = nr[pl.ds(pl.multiple_of(me_e * rows, rows), rows), :]
+    loads[base + 2].wait()
+    loads[base + 3].wait()
+    shared = (silu(dot_t(own_rows, sg[...])) * dot_t(own_rows, su[...])).astype(BF16)
+    for k in near[1:]:
+        norm_group(k)
     all_rows = nr[...]
-    base = len(first)
     loads[base].wait()
     loads[base + 1].wait()
     hidden = []
     for j in range(local_experts):
         hidden.append((silu(dot(all_rows, eg[j])) * dot(all_rows, eu[j])).astype(BF16))
-    loads[base + 2].wait()
-    loads[base + 3].wait()
-    own_rows = nr[pl.ds(pl.multiple_of(me_e * rows, rows), rows), :]
-    shared = (silu(dot(own_rows, sg[...])) * dot(own_rows, su[...])).astype(BF16)
     loads[base + 4].wait()
     loads[base + 5].wait()
     weights = [cw_col[j] for j in range(local_experts)]
-    for t in range(n_tp):
-        span = slice(t * cols, (t + 1) * cols)
+    own_span = pl.ds(pl.multiple_of(me_e * rows, rows), rows)
+    for k in list(range(1, n_tp)) + [0]:
+        peer = lax.rem(me_t + k, n_tp)
+        span = pl.ds(pl.multiple_of(peer * cols, cols), cols)
         acc = jnp.zeros((n_ep * rows, cols), F32)
         for j in range(local_experts):
             part = dot(hidden[j], ed[j, :, span]).astype(BF16).astype(F32)
             acc += weights[j] * part
-        shared_part = dot(shared, sd[:, span])
-        for g in range(n_ep):
-            mine = jnp.where(me_e == g, 1.0, 0.0)
-            block = acc[g * rows : (g + 1) * rows] + mine * shared_part
-            a2a_send[g * n_tp + t] = block.astype(BF16)
-    for k in range(1, n_all):
-        peer = lax.rem(me + k, n_all)
-        send(a2a_send.at[peer], a2a.at[me], 4, device(peer))
-    a2a[me] = a2a_send[me]
+        acc_buf[...] = acc
+        acc_buf[own_span, :] += dot(shared, sd[:, span])
+        if k:
+            a2a_send[peer] = acc_buf[...].astype(BF16)
+            send(a2a_send.at[peer], a2a.at[me_t], 4, (me_e, peer))
+        else:
+            a2a[me_t] = acc_buf[...].astype(BF16)
     start = pl.multiple_of(me_t * cols, cols)
-    own_cols = nr[pl.ds(pl.multiple_of(me_e * rows, rows), rows), pl.ds(start, cols)]
+    own_cols = nr[own_span, pl.ds(start, cols)]
+    arrived(a2a, n_tp - 1, 4)
+    plane = a2a[0].astype(F32)
+    for i in range(1, n_tp):
+        plane += a2a[i].astype(F32)
+    acc_buf[...] = plane
+    for g in range(n_ep):
+        z_send[g] = plane[g * rows : (g + 1) * rows].astype(BF16)
+    for k in range(1, n_ep):
+        peer = lax.rem(me_e + k, n_ep)
+        send(z_send.at[peer], z_recv.at[me_e], 3, (peer, me_t))
+    z_recv[me_e] = z_send[me_e]
     final = ALPHA * own_cols.astype(F32)
-    arrived(a2a, n_all - 1, 4)
-    for i in range(n_all):
-        final += a2a[i].astype(F32)
+    arrived(z_recv, n_ep - 1, 3)
+    for g in range(n_ep):
+        final += z_recv[g].astype(F32)
     mean_own = jnp.sum(final, -1, keepdims=True) / cols
     apart = final - mean_own
     spread_own = jnp.sum(apart * apart, -1, keepdims=True)
@@ -305,7 +343,6 @@
 ):
     n_tp = lax.axis_size("tp")
     n_ep = lax.axis_size("ep")
-    n_all = n_tp * n_ep
     seqs, cols = hidden_in.shape
     rows = -(-seqs // 16) * 16
     heads, head = lower_bound.shape
@@ -320,8 +357,8 @@
         exp_gate,
         exp_up,
         exp_down,
-        sh_gate,
-        sh_up,
+        sh_gate.T,
+        sh_up.T,
         sh_down,
     ]
     vmem = pl.BlockSpec(memory_space=pltpu.VMEM)
@@ -336,16 +373,20 @@
         pltpu.VMEM((heads, rows, head), F32),
         pltpu.VMEM((n_tp, rows, cols), BF16),
         pltpu.VMEM((n_tp, rows, cols), BF16),
-        pltpu.VMEM((n_all, rows, cols), BF16),
+        pltpu.VMEM((n_ep, n_tp, rows, cols), BF16),
         pltpu.VMEM((n_ep * rows, n_tp * cols), BF16),
         pltpu.VMEM((local_experts, n_ep * rows, 1), F32),
-        pltpu.VMEM((n_all, rows, cols), BF16),
-        pltpu.VMEM((n_all, rows, cols), BF16),
+        pltpu.VMEM((n_tp, n_ep * rows, cols), BF16),
+        pltpu.VMEM((n_tp, n_ep * rows, cols), BF16),
+        pltpu.VMEM((n_ep, rows, cols), BF16),
+        pltpu.VMEM((n_ep, rows, cols), BF16),
+        pltpu.VMEM((n_ep * rows, cols), F32),
+        pltpu.VMEM((128, 128), F32),
         pltpu.VMEM((n_tp, rows, 128), F32),
         pltpu.SemaphoreType.DMA((12,)),
         pltpu.SemaphoreType.DMA((heads,)),
-        pltpu.SemaphoreType.DMA((6,)),
-        pltpu.SemaphoreType.DMA((6,)),
+        pltpu.SemaphoreType.DMA((5 + 2 * n_ep,)),
+        pltpu.SemaphoreType.DMA((5 + 2 * n_ep,)),
     ]
     kernel = functools.partial(layer_kernel, n_ep, n_tp)
     row = lambda a: a.reshape(1, -1)
@@ -367,8 +408,8 @@
         row(head_gain),
         row(ln1_gain),
         row(ln1_bias),
-        routes,
-        route_weights,
+        routes.T,
+        route_weights.T,
         row(ln2_gain),
         row(ln2_bias),
         *whole,

time: 52.3 us -> 46.9 us (0.90)
  local copies, waits for them, and re-layouts: 11.8 us -> 5.2 us
  Pallas kernels: 39.5 us -> 40.8 us
    unnamed x6 -> x2, local copies, waits for them, and re-layouts: 11.8 us -> 5.2 us
    pallas_call x1, Pallas kernels: 39.5 us -> 40.8 us  [fused(): pl.pallas_call(kernel, out_shape=(jax.ShapeDtypeStruct(hidden_in.shape, B...]
where the time goes in v2:
time: 46.9 us; the launch traced here: 46.7 us
  Pallas kernels  40.8 us (87%)
  local copies, waits for them, and re-layouts  5.2 us (11%)
  between operations  0.65 us (1%)
    pallas_call x1, Pallas kernels, fused(): pl.pallas_call(kernel, out_shape=(jax.ShapeDtypeStruct(hidden_in.shape, B...  40.8 us
    unnamed x2, local copies, waits for them, and re-layouts  5.2 us

profile of v2, /device:TPU:0, one launch (start us, length us, event | category | flops | bytes accessed | tf_op | source)
XLA Modules:
  0.0 46.7 jit_solution(887542533641506164)
XLA Ops:
  0.6 40.8 %shard_map.212 = (bf16[12,256]{1,0:T(8,128)(2,1)}, f32[12,4,128,128]{3,2,1,0:T(8,128)}) custom-call(bf16[12,256]{1,0:T(8,128)(2,1)} %hid.1, f32[4,128]{1,0:T(4,128)} %lb.1, f32[1,128]{1,0:T(1,128)} %bitcast.17, f32[1,2048]{1,0:T(1,128)} %bitcast.11, f32[1,2048]{1,0:T(1,128)} %bitcast.12, s32[4,12]{1,0:T(4,128)} %bitcast.15, f32[4,12]{1,0:T(4,128)} %bitcast.16, ...), custom_call_target="tpu_custom_call" | custom-call | tf_op jit(solution)/shard_map/pallas_call | solution.py:393
  41.4 1.3 %copy.25 = bf16[12,256]{1,0:T(8,128)(2,1)} copy(bf16[12,256]{1,0:T(8,128)(2,1)} %get-tuple-element.4) | data formatting | bytes 12288
  42.7 3.9 %copy.26 = f32[12,4,128,128]{3,2,1,0:T(8,128)} copy(f32[12,4,128,128]{3,2,1,0:T(8,128)} %get-tuple-element.5) | data formatting | bytes 6291456

commit v3 on v2

--- a/solution.py
+++ b/solution.py
@@ -56,7 +56,7 @@
     su_h,
     sd_h,
     out,
-    ns_h,
+    ns,
     st,
     wf,
     wi,
@@ -88,7 +88,6 @@
     cw_t,
     stat,
     load_sem,
-    ns_sem,
     send_sem,
     recv_sem,
 ):
@@ -181,17 +180,14 @@
         vals[h] = value_in[:, span]
     loads[4].wait()
     ro[...] = jnp.zeros_like(ro)
-    outs = []
     for h in range(heads):
         for b in range(seqs):
             f_col = cols_t[h, :, b : b + 1]
             k_col = cols_t[h, :, rows + b : rows + b + 1]
             q_col = cols_t[h, :, 2 * rows + b : 2 * rows + b + 1]
             new = f_col * st[b, h] + k_col * vals[h, b : b + 1, :]
-            st[b, h] = new
+            ns[b, h] = new
             ro[h, b : b + 1, :] = jnp.sum(q_col * new, axis=0, keepdims=True)
-        outs.append(pltpu.make_async_copy(st.at[:, h], ns_h.at[:, h], ns_sem.at[h]))
-        outs[-1].start()
     mixed = []
     for h in range(heads):
         readout = ro[h]
@@ -314,8 +310,6 @@
     out[...] = result[0:seqs, :].astype(BF16)
     for copy in sends:
         copy.wait_send()
-    for copy in outs:
-        copy.wait()
 
 
 def fused(
@@ -384,7 +378,6 @@
         pltpu.VMEM((128, 128), F32),
         pltpu.VMEM((n_tp, rows, 128), F32),
         pltpu.SemaphoreType.DMA((12,)),
-        pltpu.SemaphoreType.DMA((heads,)),
         pltpu.SemaphoreType.DMA((5 + 2 * n_ep,)),
         pltpu.SemaphoreType.DMA((5 + 2 * n_ep,)),
     ]
@@ -394,13 +387,13 @@
         kernel,
         out_shape=(
             jax.ShapeDtypeStruct(hidden_in.shape, BF16),
-            jax.ShapeDtypeStruct(state.shape, F32),
+            pltpu.VMEM(state.shape, F32),
         ),
         in_specs=[vmem] * 9 + [hbm] * 12,
-        out_specs=(vmem, hbm),
+        out_specs=(vmem, vmem),
         scratch_shapes=scratch,
         compiler_params=pltpu.CompilerParams(
-            collective_id=0, has_side_effects=True, vmem_limit_bytes=60 * 1024 * 1024
+            collective_id=0, has_side_effects=True, vmem_limit_bytes=63_400_000
         ),
     )(
         hidden_in,

time: 46.9 us -> 43.8 us (0.934)
  local copies, waits for them, and re-layouts: 5.2 us -> 2.27 us
    unnamed x2 -> x4, local copies, waits for them, and re-layouts: 5.2 us -> 2.27 us
where the time goes in v3:
time: 43.8 us; the launch traced here: 43.6 us
  Pallas kernels  40.7 us (93%)
  local copies, waits for them, and re-layouts  2.27 us (5%)
  between operations  0.66 us (2%)
    pallas_call x1, Pallas kernels, fused(): pl.pallas_call(kernel, out_shape=(jax.ShapeDtypeStruct(hidden_in.shape, B...  40.7 us
    unnamed x4, local copies, waits for them, and re-layouts  2.27 us

profile of v3, /device:TPU:0, one launch (start us, length us, event | category | flops | bytes accessed | tf_op | source)
XLA Modules:
  0.0 43.6 jit_solution(7798763579704149628)
XLA Ops:
  0.6 40.7 %shard_map.212 = (bf16[12,256]{1,0:T(8,128)(2,1)}, f32[12,4,128,128]{3,2,1,0:T(8,128)S(1)}) custom-call(bf16[12,256]{1,0:T(8,128)(2,1)} %hid.1, f32[4,128]{1,0:T(4,128)} %lb.1, f32[1,128]{1,0:T(1,128)} %bitcast.17, f32[1,2048]{1,0:T(1,128)} %bitcast.11, f32[1,2048]{1,0:T(1,128)} %bitcast.12, s32[4,12]{1,0:T(4,128)} %bitcast.15, f32[4,12]{1,0:T(4,128)} %bitcast.16, ...), custom_call_target="tpu_custom_call" | custom-call | tf_op jit(solution)/shard_map/pallas_call | solution.py:386
  41.3 0.0 copy-start
  41.3 1.7 %copy.25 = f32[12,4,128,128]{3,2,1,0:T(8,128)} copy(f32[12,4,128,128]{3,2,1,0:T(8,128)S(1)} %get-tuple-element.3) | data formatting | bytes 6291456
  43.0 0.0 copy-done
  43.0 0.6 %copy.26 = bf16[12,256]{1,0:T(8,128)(2,1)} copy(bf16[12,256]{1,0:T(8,128)(2,1)S(1)} %copy-done) | data formatting | bytes 12288
Async XLA Ops:
  41.3 1.7 %copy-start = (bf16[12,256]{1,0:T(8,128)(2,1)S(1)}, bf16[12,256]{1,0:T(8,128)(2,1)}, u32[]{:S(2)}) copy-start(bf16[12,256]{1,0:T(8,128)(2,1)} %get-tuple-element.6) | copy-start | bytes 18436

commit v4 on v3

--- a/solution.py
+++ b/solution.py
@@ -230,27 +230,31 @@
         centered = row - jnp.sum(row, -1, keepdims=True) / width
         variance = jnp.sum(centered * centered, -1, keepdims=True) / width
         normed = centered * lax.rsqrt(variance + EPS) * g1[...] + b1[...]
-        nr[pl.ds(pl.multiple_of(group * rows, rows), rows), :] = normed.astype(BF16)
+        return normed[0:seqs]
 
     forward(0)
     arrived(cws, n_ep - 1, 1)
-    for g in range(n_ep):
+    for k in range(n_ep):
+        table = cws[lax.rem(me_e + n_ep - k, n_ep)]
+        at = lax.broadcasted_iota(jnp.int32, table.shape, 1)
         for j in range(local_experts):
-            at = lax.broadcasted_iota(jnp.int32, cws.shape[1:], 1)
-            cw_col[j, g * rows : (g + 1) * rows, :] = jnp.sum(
-                jnp.where(at == me_e * local_experts + j, cws[g], 0.0), axis=1, keepdims=True
+            column = jnp.where(at == me_e * local_experts + j, table, 0.0)
+            cw_col[j, k * seqs : (k + 1) * seqs, :] = jnp.sum(
+                column[0:seqs], axis=1, keepdims=True
             )
     base = len(first)
     for k in near[1:]:
         forward(k)
-    norm_group(0)
-    own_rows = nr[pl.ds(pl.multiple_of(me_e * rows, rows), rows), :]
+    own_normed = norm_group(0)
+    nr[0:seqs, :] = own_normed
+    nr[seqs:rows, :] = jnp.zeros((rows - seqs, width), F32)
+    own_rows = nr[0:rows, :].astype(BF16)
     loads[base + 2].wait()
     loads[base + 3].wait()
     shared = (silu(dot_t(own_rows, sg[...])) * dot_t(own_rows, su[...])).astype(BF16)
     for k in near[1:]:
-        norm_group(k)
-    all_rows = nr[...]
+        nr[k * seqs : (k + 1) * seqs, :] = norm_group(k)
+    all_rows = nr[...].astype(BF16)
     loads[base].wait()
     loads[base + 1].wait()
     hidden = []
@@ -259,34 +263,34 @@
     loads[base + 4].wait()
     loads[base + 5].wait()
     weights = [cw_col[j] for j in range(local_experts)]
-    own_span = pl.ds(pl.multiple_of(me_e * rows, rows), rows)
     for k in list(range(1, n_tp)) + [0]:
         peer = lax.rem(me_t + k, n_tp)
         span = pl.ds(pl.multiple_of(peer * cols, cols), cols)
-        acc = jnp.zeros((n_ep * rows, cols), F32)
+        acc = jnp.zeros(acc_buf.shape, F32)
         for j in range(local_experts):
             part = dot(hidden[j], ed[j, :, span]).astype(BF16).astype(F32)
             acc += weights[j] * part
         acc_buf[...] = acc
-        acc_buf[own_span, :] += dot(shared, sd[:, span])
+        acc_buf[0:seqs, :] += dot(shared, sd[:, span])[0:seqs]
         if k:
             a2a_send[peer] = acc_buf[...].astype(BF16)
             send(a2a_send.at[peer], a2a.at[me_t], 4, (me_e, peer))
         else:
             a2a[me_t] = acc_buf[...].astype(BF16)
     start = pl.multiple_of(me_t * cols, cols)
-    own_cols = nr[own_span, pl.ds(start, cols)]
+    xf[0:seqs, :] = nr[0:seqs, pl.ds(start, cols)]
+    own_cols = xf[...].astype(BF16)
     arrived(a2a, n_tp - 1, 4)
     plane = a2a[0].astype(F32)
     for i in range(1, n_tp):
         plane += a2a[i].astype(F32)
-    acc_buf[...] = plane
-    for g in range(n_ep):
-        z_send[g] = plane[g * rows : (g + 1) * rows].astype(BF16)
-    for k in range(1, n_ep):
-        peer = lax.rem(me_e + k, n_ep)
-        send(z_send.at[peer], z_recv.at[me_e], 3, (peer, me_t))
-    z_recv[me_e] = z_send[me_e]
+    for k in reversed(near[1:]):
+        xf[0:seqs, :] = plane[k * seqs : (k + 1) * seqs]
+        z_send[k] = xf[...].astype(BF16)
+        peer = lax.rem(me_e + n_ep - k, n_ep)
+        send(z_send.at[k], z_recv.at[me_e], 3, (peer, me_t))
+    xf[0:seqs, :] = plane[0:seqs]
+    z_recv[me_e] = xf[...].astype(BF16)
     final = ALPHA * own_cols.astype(F32)
     arrived(z_recv, n_ep - 1, 3)
     for g in range(n_ep):
@@ -368,13 +372,13 @@
         pltpu.VMEM((n_tp, rows, cols), BF16),
         pltpu.VMEM((n_tp, rows, cols), BF16),
         pltpu.VMEM((n_ep, n_tp, rows, cols), BF16),
-        pltpu.VMEM((n_ep * rows, n_tp * cols), BF16),
-        pltpu.VMEM((local_experts, n_ep * rows, 1), F32),
-        pltpu.VMEM((n_tp, n_ep * rows, cols), BF16),
-        pltpu.VMEM((n_tp, n_ep * rows, cols), BF16),
+        pltpu.VMEM((n_ep * seqs, n_tp * cols), F32),
+        pltpu.VMEM((local_experts, n_ep * seqs, 1), F32),
+        pltpu.VMEM((n_tp, n_ep * seqs, cols), BF16),
+        pltpu.VMEM((n_tp, n_ep * seqs, cols), BF16),
         pltpu.VMEM((n_ep, rows, cols), BF16),
         pltpu.VMEM((n_ep, rows, cols), BF16),
-        pltpu.VMEM((n_ep * rows, cols), F32),
+        pltpu.VMEM((n_ep * seqs, cols), F32),
         pltpu.VMEM((128, 128), F32),
         pltpu.VMEM((n_tp, rows, 128), F32),
         pltpu.SemaphoreType.DMA((12,)),
@@ -419,6 +423,7 @@
     return (
         cols % 128 == 0
         and seqs <= 16
+        and n_ep * seqs % 16 == 0
         and state.shape[2] == 128
         and exp_gate.shape[0] <= 128
         and n_tp * n_ep <= 64

time: 43.8 us -> 43.4 us (level)
  no operation moved by 1% of the time
where the time goes in v4:
time: 43.4 us; the launch traced here: 43.2 us
  Pallas kernels  40.3 us (93%)
  local copies, waits for them, and re-layouts  2.27 us (5%)
  between operations  0.66 us (2%)
    pallas_call x1, Pallas kernels, fused(): pl.pallas_call(kernel, out_shape=(jax.ShapeDtypeStruct(hidden_in.shape, B...  40.3 us
    unnamed x4, local copies, waits for them, and re-layouts  2.27 us

profile of v4, /device:TPU:0, one launch (start us, length us, event | category | flops | bytes accessed | tf_op | source)
XLA Modules:
  0.0 43.2 jit_solution(3902968564204416088)
XLA Ops:
  0.6 40.3 %shard_map.212 = (bf16[12,256]{1,0:T(8,128)(2,1)}, f32[12,4,128,128]{3,2,1,0:T(8,128)S(1)}) custom-call(bf16[12,256]{1,0:T(8,128)(2,1)} %hid.1, f32[4,128]{1,0:T(4,128)} %lb.1, f32[1,128]{1,0:T(1,128)} %bitcast.17, f32[1,2048]{1,0:T(1,128)} %bitcast.11, f32[1,2048]{1,0:T(1,128)} %bitcast.12, s32[4,12]{1,0:T(4,128)} %bitcast.15, f32[4,12]{1,0:T(4,128)} %bitcast.16, ...), custom_call_target="tpu_custom_call" | custom-call | tf_op jit(solution)/shard_map/pallas_call | solution.py:390
  40.9 0.0 copy-start
  40.9 1.7 %copy.25 = f32[12,4,128,128]{3,2,1,0:T(8,128)} copy(f32[12,4,128,128]{3,2,1,0:T(8,128)S(1)} %get-tuple-element.3) | data formatting | bytes 6291456
  42.6 0.0 copy-done
  42.6 0.6 %copy.26 = bf16[12,256]{1,0:T(8,128)(2,1)} copy(bf16[12,256]{1,0:T(8,128)(2,1)S(1)} %copy-done) | data formatting | bytes 12288
Async XLA Ops:
  40.9 1.7 %copy-start = (bf16[12,256]{1,0:T(8,128)(2,1)S(1)}, bf16[12,256]{1,0:T(8,128)(2,1)}, u32[]{:S(2)}) copy-start(bf16[12,256]{1,0:T(8,128)(2,1)} %get-tuple-element.6) | copy-start | bytes 18436
